TPU v7x, 32 devices: a whole 2x2x4 slice. The times are simulated.
32 devices in a mesh: fs: 2 (over core), tp: 16 (over z, y, x).
Axes of the slice: x: 2, y: 2, z: 4, core: 2. Of those that a mesh axis runs over, the one named last changes fastest.
Arguments:
- trained_gate: float32 [16, 504, 2048], P(None, 'fs', 'tp'), may hold values from -0.125 to 0.125
- trained_up: float32 [16, 504, 2048], P(None, 'fs', 'tp'), may hold values from -0.125 to 0.125
- trained_down: float32 [16, 504, 2048], P(None, 'fs', 'tp'), may hold values from -0.25 to 0.25
- trained_shared_gate: float32 [504, 2048], P('fs', 'tp'), may hold values from -0.125 to 0.125
- trained_shared_up: float32 [504, 2048], P('fs', 'tp'), may hold values from -0.125 to 0.125
- trained_shared_down: float32 [504, 2048], P('fs', 'tp'), may hold values from -0.25 to 0.25
- ffn_gain: float32 [2048], P('tp'), may hold values from 0.1 to 1.9
- prompt_tokens: bfloat16 [512, 2048], P('fs'), may hold values from -6 to 6
- expert_ids: int32 [512, 8], P('fs'), may hold values from 0 to 15, all different within a row; in each aligned block of 256 rows (0 to 255, 256 to 511, ...) at most 256 rows name the same one
- route_scores: float32 [512, 8], P('fs'), may hold values from 0.05 to 1
Outputs:
- served_gate: bfloat16 [16, 504, 2048], P('tp')
- served_up: bfloat16 [16, 504, 2048], P('tp')
- served_down: bfloat16 [16, 504, 2048], P('tp')
- served_shared_gate: bfloat16 [504, 2048], P(None, 'tp')
- served_shared_up: bfloat16 [504, 2048], P(None, 'tp')
- served_shared_down: bfloat16 [504, 2048], P(None, 'tp')
- mixture_out: bfloat16 [512, 2048], P('fs', 'tp')
Inputs may be any that keep to these rules, and one draw needn't show every extreme that they name: `expert_ids`: each row names 8 different experts, and every expert is named by some row. Within the 256 rows of one index of fs no expert is named by more than 256 rows, and in every draw some expert is named by exactly 256 rows of some index of fs.
All inputs are finite; a program needn't handle non-finite values.
Results may differ from a plain program's by a relative error of at most 0.0082.
Values may be sent and summed in bfloat16 or wider, within the bound.
No kernel may reach another device: no remote copies, remote signals or barrier semaphores. Data moves between devices by JAX's collectives and lax.ppermute only.
A program may use at most 64 MiB of HBM per device.

v0:
```python
import jax
import jax.numpy as jnp
from jax import lax
from jax.sharding import PartitionSpec as P

EPSILON = 1e-06
ROUTED_SCALE = 2.5


def contract(left, right):
    return lax.dot_general(
        left, right, (((1,), (1,)), ((), ())), preferred_element_type=jnp.float32
    )


def on_device(
    trained_gate,
    trained_up,
    trained_down,
    trained_shared_gate,
    trained_shared_up,
    trained_shared_down,
    ffn_gain,
    prompt_tokens,
    expert_ids,
    route_scores,
):
    gate_cast = (trained_gate * ffn_gain[None, None, :]).astype(jnp.bfloat16)
    up_cast = (trained_up * ffn_gain[None, None, :]).astype(jnp.bfloat16)
    down_cast = trained_down.astype(jnp.bfloat16)
    shared_gate_cast = (trained_shared_gate * ffn_gain[None, :]).astype(jnp.bfloat16)[None]
    shared_up_cast = (trained_shared_up * ffn_gain[None, :]).astype(jnp.bfloat16)[None]
    shared_down_cast = trained_shared_down.astype(jnp.bfloat16)[None]
    expert_gate, expert_up, expert_down = (
        lax.all_to_all(gate_cast, "tp", split_axis=0, concat_axis=2, tiled=True),
        lax.all_to_all(up_cast, "tp", split_axis=0, concat_axis=2, tiled=True),
        lax.all_to_all(down_cast, "tp", split_axis=0, concat_axis=2, tiled=True),
    )
    token_count, model_width = prompt_tokens.shape
    tokens_float = prompt_tokens.astype(jnp.float32)
    normed = (
        tokens_float
        * lax.rsqrt(jnp.mean(tokens_float * tokens_float, axis=1, keepdims=True) + EPSILON)
    ).astype(jnp.bfloat16)
    column_width = ffn_gain.shape[0]
    expert_index = lax.axis_index("tp")
    normed_cols = lax.dynamic_slice_in_dim(normed, expert_index * column_width, column_width, 1)
    expert_count = lax.axis_size("tp")
    top_count = expert_ids.shape[1]
    capacity = min(token_count, 5 * token_count * top_count // (2 * expert_count))
    route_weight = ROUTED_SCALE * route_scores / jnp.sum(route_scores, axis=1, keepdims=True)
    chosen = expert_ids == expert_index
    present = jnp.any(chosen, axis=1)
    position = jnp.cumsum(present.astype(jnp.int32)) - 1
    slot_match = (position[None, :] == jnp.arange(capacity, dtype=jnp.int32)[:, None]) & present[
        None, :
    ]
    slot_token = jnp.sum(
        jnp.where(slot_match, jnp.arange(token_count, dtype=jnp.int32)[None, :], 0), axis=1
    )
    slot_rows = jnp.take(normed, slot_token, axis=0)
    gathered = (
        lax.all_gather(expert_gate, "fs", axis=1, tiled=True),
        lax.all_gather(expert_up, "fs", axis=1, tiled=True),
        lax.all_gather(expert_down, "fs", axis=1, tiled=True),
        lax.all_gather(shared_gate_cast, "fs", axis=1, tiled=True),
        lax.all_gather(shared_up_cast, "fs", axis=1, tiled=True),
        lax.all_gather(shared_down_cast, "fs", axis=1, tiled=True),
    )
    gate_full, up_full, down_full, sgate_full, sup_full, sdown_full = gathered
    gate_pre = contract(slot_rows, gate_full[0])
    up_pre = contract(slot_rows, up_full[0])
    sgate_part = contract(normed_cols, sgate_full[0])
    sup_part = contract(normed_cols, sup_full[0])
    expert_act = (jax.nn.silu(gate_pre) * up_pre).astype(jnp.bfloat16)
    shared_gate_pre, shared_up_pre = lax.psum((sgate_part, sup_part), "tp")
    shared_act = (jax.nn.silu(shared_gate_pre) * shared_up_pre).astype(jnp.bfloat16)
    expert_out = jnp.dot(expert_act, down_full[0], preferred_element_type=jnp.float32)
    shared_out = jnp.dot(shared_act, sdown_full[0], preferred_element_type=jnp.float32)
    arrived = lax.all_to_all(expert_out, "tp", split_axis=1, concat_axis=0, tiled=True)
    arrived = arrived.reshape(expert_count, capacity, column_width)

    def add_expert(total, inputs):
        source_index, source_rows = inputs
        source_chosen = expert_ids == source_index
        source_weight = jnp.sum(jnp.where(source_chosen, route_weight, 0.0), axis=1)
        source_present = jnp.any(source_chosen, axis=1)
        source_position = jnp.cumsum(source_present.astype(jnp.int32)) - 1
        source_picked = jnp.take(source_rows, jnp.maximum(source_position, 0), axis=0)
        return (
            total + jnp.where(source_present[:, None], source_picked * source_weight[:, None], 0.0),
            None,
        )

    routed_cols, _ = lax.scan(
        add_expert,
        jnp.zeros((token_count, column_width), jnp.float32),
        (jnp.arange(expert_count, dtype=jnp.int32), arrived),
    )
    mixture = (routed_cols + shared_out).astype(jnp.bfloat16)
    return (gate_full, up_full, down_full, sgate_full[0], sup_full[0], sdown_full[0], mixture)


def solution(mesh):
    placed = (
        P(None, "fs", "tp"),
        P(None, "fs", "tp"),
        P(None, "fs", "tp"),
        P("fs", "tp"),
        P("fs", "tp"),
        P("fs", "tp"),
        P("tp"),
        P("fs", None),
        P("fs", None),
        P("fs", None),
    )
    return jax.shard_map(
        on_device,
        mesh=mesh,
        in_specs=placed,
        out_specs=(
            P("tp", None, None),
            P("tp", None, None),
            P("tp", None, None),
            P(None, "tp"),
            P(None, "tp"),
            P(None, "tp"),
            P("fs", "tp"),
        ),
        check_vma=False,
    )
```

profile of v0, /device:TPU:0, one launch (start us, length us, event | category | flops | bytes accessed | tf_op | source)
XLA Modules:
  0.0 302.3 jit_solution(17603221546341830678)
XLA Ops:
  8.0 2.5 multiply_convert_fusion
  10.9 34.5 %all_to_all.67 = bf16[16,252,128]{2,1,0:T(8,128)(2,1)S(1)} all-to-all(bf16[16,252,128]{2,1,0:T(8,128)(2,1)S(1)} %copy.55), channel_id=1, replica_groups=mesh['fs'=2,'tp'=16] {'tp'}, dimensions={0} | all-to-all | bytes 2064384 | tf_op jit(solution)/shard_map/all_to_all | solution.py:35
  45.9 3.7 %copy.57 = bf16[1,252,2048]{2,0,1:T(2,128)(2,1)} copy(bf16[1,252,2048]{1,2,0:T(8,128)(2,1)S(1)} %bitcast.74) | data formatting | bytes 2064384 | tf_op jit(solution)/shard_map/all_to_all | solution.py:35
  49.9 29.4 %all_to_all.68 = bf16[16,252,128]{2,1,0:T(8,128)(2,1)S(1)} all-to-all(bf16[16,252,128]{2,1,0:T(8,128)(2,1)S(1)} %copy.58), channel_id=1, replica_groups=mesh['fs'=2,'tp'=16] {'tp'}, dimensions={0} | all-to-all | bytes 2064384 | tf_op jit(solution)/shard_map/all_to_all | solution.py:36
  79.9 3.7 %copy.60 = bf16[1,252,2048]{2,0,1:T(2,128)(2,1)} copy(bf16[1,252,2048]{1,2,0:T(8,128)(2,1)S(1)} %bitcast.75) | data formatting | bytes 2064384 | tf_op jit(solution)/shard_map/all_to_all | solution.py:36
  83.8 1.2 copy.61
  85.1 3.9 %all-to-all-start.2 = ((bf16[16,252,128]{2,1,0:T(8,128)(2,1)}), bf16[16,252,128]{2,1,0:T(8,128)(2,1)S(1)}, u32[]{:S(2)}, u32[]{:S(2)}) async-start(bf16[16,252,128]{2,1,0:T(8,128)(2,1)} %copy.61), calls=%async_computation.2 | async-start | bytes 2097152 | tf_op jit(solution)/shard_map/all_to_all | solution.py:37
  89.6 23.0 %all-to-all-done.2 = bf16[16,252,128]{2,1,0:T(8,128)(2,1)S(1)} async-done(((bf16[16,252,128]{2,1,0:T(8,128)(2,1)}), bf16[16,252,128]{2,1,0:T(8,128)(2,1)S(1)}, u32[]{:S(2)}, u32[]{:S(2)}) %all-to-all-start.2) | async-done | bytes 1032224 | tf_op jit(solution)/shard_map/all_to_all | solution.py:37
  113.1 3.9 %copy.63 = bf16[1,252,2048]{2,0,1:T(2,128)(2,1)} copy(bf16[1,252,2048]{1,2,0:T(8,128)(2,1)S(1)} %bitcast.76) | data formatting | bytes 2064384 | tf_op jit(solution)/shard_map/all_to_all | solution.py:37
  117.9 2.3 gather_fusion.1
  120.2 3.4 %copy.66 = bf16[1,504,2048]{2,1,0:T(8,128)(2,1)S(1)} copy(bf16[1,504,2048]{2,0,1:T(2,128)(2,1)} %all-gather.10.cloned.1.call-done) | data formatting | bytes 4128768
  123.7 6.1 %copy.67 = bf16[1,504,2048]{2,1,0:T(8,128)(2,1)} copy(bf16[1,504,2048]{2,0,1:T(2,128)(2,1)} %all-gather.12.cloned.1.call-done) | data formatting | bytes 4128768
  129.8 1.6 fusion.4
  131.4 9.0 %copy.73 = bf16[1,504,2048]{1,2,0:T(8,128)(2,1)S(1)} copy(bf16[1,504,2048]{2,0,1:T(2,128)(2,1)} %all-gather.14.cloned.1.call-done) | data formatting | bytes 4128768 | tf_op jit(solution)/shard_map/dot_general | solution.py:78
  140.4 5.8 %fusion.17 = f32[256,16,128]{2,0,1:T(8,128)} fusion(bf16[16,128,504]{2,1,0:T(8,128)(2,1)S(1)} %bitcast.78, bf16[1,504,2048]{2,1,0:T(8,128)(2,1)} %copy.67, f32[256,504]{0,1:T(8,128)} %fusion.4, bf16[256,2048]{1,0:T(8,128)(2,1)} %gather_fusion.1, pred[256]{0:T(512)(128)(4,1)S(1)} %compare_and_fusion), kind=kOutput, calls=%fused_computation.27 | convolution fusion | flops 1058263040 | bytes 7790848 | tf_op jit(solution)/shard_map/dot_general | solution.py:78
  146.2 6.6 %all-to-all-start.3 = ((f32[256,16,128]{2,0,1:T(8,128)}), f32[256,16,128]{2,0,1:T(8,128)S(1)}, u32[]{:S(2)}, u32[]{:S(2)}) async-start(f32[256,16,128]{2,0,1:T(8,128)} %fusion.17), calls=%async_computation.3 | async-start | bytes 4194304 | tf_op jit(solution)/shard_map/all_to_all | solution.py:80
  153.0 1.9 all-gather.3
  154.9 1.9 all-gather.4
  159.1 2.1 all-gather.5
  161.2 4.8 %copy.68 = bf16[1,504,2048]{2,1,0:T(8,128)(2,1)} copy(bf16[1,504,2048]{2,0,1:T(2,128)(2,1)} %all-gather.14.cloned.1.call-done) | data formatting | bytes 4128768
  166.0 38.5 %all-to-all-done.3 = f32[256,16,128]{2,0,1:T(8,128)S(1)} async-done(((f32[256,16,128]{2,0,1:T(8,128)}), f32[256,16,128]{2,0,1:T(8,128)S(1)}, u32[]{:S(2)}, u32[]{:S(2)}) %all-to-all-start.3) | async-done | bytes 2097184 | tf_op jit(solution)/shard_map/all_to_all | solution.py:80
  204.4 47.8 %while.13 = (s32[]{:T(128)}, f32[256,128]{1,0:T(8,128)S(1)}, s32[16]{0:T(128)S(1)}, s32[256,8]{0,1:T(8,128)S(1)}, f32[16,256,128]{2,1,0:T(8,128)S(1)}, /*index=5...) while((s32[]{:T(128)}, f32[256,128]{1,0:T(8,128)S(1)}, s32[16]{0:T(128)S(1)}, ...), condition=%wide.region_11.12_spmd.clone, body=%wide.region_6.11_spmd.clone.sunk | while | flops 206342 | bytes 952776 | solution.py:95
  252.2 40.8 %all-reduce.3.cloned.1.call-done = (f32[256,504]{0,1:T(8,128)}, f32[256,504]{0,1:T(8,128)}) async-done(((f32[256,504]{0,1:T(8,128)}, f32[256,504]{0,1:T(8,128)}), (f32[256,504]{0,1:T(8,128)}, f32[256,504]{0,1:T(8,128)})) %all-reduce.3.cloned.1.call-update) | async-done | bytes 1032208 | tf_op jit(solution)/shard_map/psum | solution.py:76
  293.0 2.2 fusion.15
  (276 shorter events, 53.3 us)
Async XLA Ops:
  8.0 112.2 %all-gather.10.cloned.1.call-start = ((), (), s32[]{:S(2)}) async-start(), calls=%async_computation.4 | async-start | bytes 6193152 | tf_op jit(solution)/shard_map/all_gather | solution.py:63
  49.6 74.1 %all-gather.12.cloned.1.call-start = ((), (), s32[]{:S(2)}) async-start(), calls=%async_computation.5 | async-start | bytes 6193152 | tf_op jit(solution)/shard_map/all_gather | solution.py:64
  79.9 3.8 %copy-start.2 = (f32[16,252,128]{2,0,1:T(8,128)S(1)}, f32[16,252,128]{2,0,1:T(8,128)}, u32[]{:S(2)}) copy-start(f32[16,252,128]{2,0,1:T(8,128)} %param.14) | copy-start | bytes 6193156
  83.8 5.2 %copy-start.6 = (s32[256,8]{0,1:T(8,128)S(1)}, s32[256,8]{0,1:T(8,128)}, u32[]{:S(2)}) copy-start(s32[256,8]{0,1:T(8,128)} %param.20) | copy-start | bytes 24580
  85.1 27.5 %all-to-all-start.2 = ((bf16[16,252,128]{2,1,0:T(8,128)(2,1)}), bf16[16,252,128]{2,1,0:T(8,128)(2,1)S(1)}, u32[]{:S(2)}, u32[]{:S(2)}) async-start(bf16[16,252,128]{2,1,0:T(8,128)(2,1)} %copy.61), calls=%async_computation.2 | async-start | bytes 2097152 | tf_op jit(solution)/shard_map/all_to_all | solution.py:37
  89.0 42.4 %all-gather.14.cloned.1.call-start = ((), (), s32[]{:S(2)}) async-start(), calls=%async_computation.6 | async-start | bytes 6193152 | tf_op jit(solution)/shard_map/all_gather | solution.py:65
  113.1 4.2 %copy-start = (bf16[256,2048]{1,0:T(8,128)(2,1)S(1)}, bf16[256,2048]{1,0:T(8,128)(2,1)}, u32[]{:S(2)}) copy-start(bf16[256,2048]{1,0:T(8,128)(2,1)} %param.19) | copy-start | bytes 3145732
  123.6 6.1 %copy-start.1 = (bf16[1,504,2048]{2,1,0:T(8,128)(2,1)}, bf16[1,504,2048]{2,1,0:T(8,128)(2,1)S(1)}, u32[]{:S(2)}) copy-start(bf16[1,504,2048]{2,1,0:T(8,128)(2,1)S(1)} %copy.66) | copy-start | bytes 6193156
  123.7 6.1 %copy-start.3 = (bf16[256,2048]{1,0:T(8,128)(2,1)S(1)}, bf16[256,2048]{1,0:T(8,128)(2,1)}, u32[]{:S(2)}) copy-start(bf16[256,2048]{1,0:T(8,128)(2,1)} %gather_fusion.1) | copy-start | bytes 3145732
  146.2 6.7 %copy-start.8 = (f32[252,128]{1,0:T(8,128)S(1)}, f32[252,128]{1,0:T(8,128)}, u32[]{:S(2)}) copy-start(f32[252,128]{1,0:T(8,128)} %param.16) | copy-start | bytes 387076
  146.2 6.7 %copy-start.9 = (f32[252,128]{1,0:T(8,128)S(1)}, f32[252,128]{1,0:T(8,128)}, u32[]{:S(2)}) copy-start(f32[252,128]{1,0:T(8,128)} %param.15) | copy-start | bytes 387076
  146.2 6.7 %copy-start.12 = (f32[128]{0:T(128)S(1)}, f32[128]{0:T(128)}, u32[]{:S(2)}) copy-start(f32[128]{0:T(128)} %param.18) | copy-start | bytes 1540
  146.2 58.2 %all-to-all-start.3 = ((f32[256,16,128]{2,0,1:T(8,128)}), f32[256,16,128]{2,0,1:T(8,128)S(1)}, u32[]{:S(2)}, u32[]{:S(2)}) async-start(f32[256,16,128]{2,0,1:T(8,128)} %fusion.17), calls=%async_computation.3 | async-start | bytes 4194304 | tf_op jit(solution)/shard_map/all_to_all | solution.py:80
  152.8 140.2 %all-reduce.3.cloned.1.call-start = ((), (), s32[]{:S(2)}) async-start(), calls=%async_computation.7 | async-start | bytes 2064384 | tf_op jit(solution)/shard_map/psum | solution.py:76
  152.9 8.2 %copy-start.11 = (f32[256,8]{0,1:T(8,128)S(1)}, f32[256,8]{0,1:T(8,128)}, u32[]{:S(2)}) copy-start(f32[256,8]{0,1:T(8,128)} %param.21) | copy-start | bytes 24580
  154.9 11.1 %copy-start.4 = (bf16[504,128]{1,0:T(8,128)(2,1)}, bf16[504,128]{1,0:T(8,128)(2,1)S(1)}, u32[]{:S(2)}) copy-start(bf16[504,128]{1,0:T(8,128)(2,1)S(1)} %reshape.181) | copy-start | bytes 387076
  156.8 9.1 %copy-start.5 = (bf16[504,128]{1,0:T(8,128)(2,1)}, bf16[504,128]{1,0:T(8,128)(2,1)S(1)}, u32[]{:S(2)}) copy-start(bf16[504,128]{1,0:T(8,128)(2,1)S(1)} %reshape.183) | copy-start | bytes 387076
  156.8 2.2 copy-start.7
  161.2 131.8 %copy-start.10 = (bf16[504,128]{1,0:T(8,128)(2,1)}, bf16[504,128]{1,0:T(8,128)(2,1)S(1)}, u32[]{:S(2)}) copy-start(bf16[504,128]{1,0:T(8,128)(2,1)S(1)} %reshape.185) | copy-start | bytes 387076
Sparse Core Ops, SparseCore 0:
  49.7 11.8 all-gather.9
  83.8 11.8 all-gather.11
  117.2 13.8 all-gather.13
Sparse Core Ops, SparseCore 1:
  159.1 133.8 all-reduce.2
where the time goes:
time: 303 us; the launch traced here: 302 us
  waiting for transfers between devices  102 us (34%)
  blocking collectives  69.7 us (23%)
  local copies, waits for them, and re-layouts  66.4 us (22%)
  other arithmetic  25.3 us (8%)
  between operations  15.5 us (5%)
  matrix products  11.7 us (4%)
  starting transfers between devices  10.7 us (4%)
    psum x1, waiting for transfers between devices, on_device(): shared_gate_pre, shared_up_pre = lax.psum((sgate_part, sup_part), 'tp')  40.8 us
    all_to_all x1, waiting for transfers between devices, on_device(): lax.all_to_all(expert_out, 'tp', split_axis=1, concat_axis=0, tiled=True)  38.5 us
    all_to_all x1, blocking collectives, on_device(): lax.all_to_all(gate_cast, 'tp', split_axis=0, concat_axis=2, tiled=True)  34.5 us
    all_to_all x1, blocking collectives, on_device(): lax.all_to_all(up_cast, 'tp', split_axis=0, concat_axis=2, tiled=True)  29.4 us
    all_to_all x1, waiting for transfers between devices, on_device(): lax.all_to_all(down_cast, 'tp', split_axis=0, concat_axis=2, tiled=True)  23 us
    unnamed x32, local copies, waits for them, and re-layouts  14.4 us
    gather x16, local copies, waits for them, and re-layouts, add_expert(): jnp.take(source_rows, jnp.maximum(source_position, 0), axis=0)  11.7 us
    reduce_sum x16, other arithmetic, add_expert(): source_weight = jnp.sum(jnp.where(source_chosen, route_weight, 0.0), axis=1)  11.3 us
  transfers between devices with their start and end apart: 6, of which 3 were waited for; matrix products, arithmetic and copies ran while one was open for 26% of the time, Pallas kernels for 0%

commit v1 on v0

--- a/solution.py
+++ b/solution.py
@@ -1,3 +1,4 @@
+import functools
 import jax
 import jax.numpy as jnp
 from jax import lax
@@ -5,6 +6,33 @@
 
 EPSILON = 1e-06
 ROUTED_SCALE = 2.5
+
+
+def spots_supply(u, along_axis, array_axis, row_dim):
+    high = lax.axis_size(along_axis)
+    then = lax.axis_index(along_axis)
+    formed, near = (high, then)
+    left_arr = u.shape[array_axis] // formed
+    ready = list(u.shape)
+    ready[array_axis] = left_arr
+    back = ready[row_dim]
+    ready[row_dim] = back * formed
+    built = jnp.zeros(ready, u.dtype)
+    for dev_j in tuple(range(formed)):
+        next_value = lax.dynamic_slice_in_dim(
+            u, (near ^ dev_j) * left_arr, left_arr, axis=array_axis
+        )
+        if dev_j:
+            next_value = lax.ppermute(
+                next_value, along_axis, perm=[(s, s ^ dev_j) for s in range(formed)]
+            )
+        built = lax.dynamic_update_slice_in_dim(
+            built, next_value, (near ^ dev_j) * back, axis=row_dim
+        )
+    return built
+
+
+_keep_up_tails = functools.partial(spots_supply, along_axis="tp", array_axis=0, row_dim=2)
 
 
 def contract(left, right):
@@ -32,7 +60,7 @@
     shared_up_cast = (trained_shared_up * ffn_gain[None, :]).astype(jnp.bfloat16)[None]
     shared_down_cast = trained_shared_down.astype(jnp.bfloat16)[None]
     expert_gate, expert_up, expert_down = (
-        lax.all_to_all(gate_cast, "tp", split_axis=0, concat_axis=2, tiled=True),
+        _keep_up_tails(gate_cast),
         lax.all_to_all(up_cast, "tp", split_axis=0, concat_axis=2, tiled=True),
         lax.all_to_all(down_cast, "tp", split_axis=0, concat_axis=2, tiled=True),
     )

time: 303 us -> 332 us (1.096)
  starting transfers between devices: 10.7 us -> 45.8 us
  blocking collectives: 69.7 us -> 41.3 us
  waiting for transfers between devices: 102 us -> 117 us
  local copies, waits for them, and re-layouts: 66.4 us -> 74.5 us
    ppermute x0 -> x15, starting transfers between devices: none -> 34.9 us  [spots_supply(): lax.ppermute(next_value, along_axis, perm=[(s, s ^ dev_j) for s in range(...]
    all_to_all x1 -> x0, blocking collectives: 34.5 us -> none  [on_device(): lax.all_to_all(gate_cast, 'tp', split_axis=0, concat_axis=2, tiled=True)]
    ppermute x0 -> x15, waiting for transfers between devices: none -> 12.7 us  [spots_supply(): lax.ppermute(next_value, along_axis, perm=[(s, s ^ dev_j) for s in range(...]
    dynamic_update_slice x0 -> x15, local copies, waits for them, and re-layouts: none -> 7.86 us  [spots_supply(): lax.dynamic_update_slice_in_dim(built, next_value, (near ^ dev_j) * back,...]
    all_to_all x1, blocking collectives: 29.4 us -> 35.6 us  [on_device(): lax.all_to_all(up_cast, 'tp', split_axis=0, concat_axis=2, tiled=True)]
    all_to_all x2 -> x0, local copies, waits for them, and re-layouts: 4.26 us -> none  [on_device(): lax.all_to_all(gate_cast, 'tp', split_axis=0, concat_axis=2, tiled=True)]
    unnamed x32 -> x34, local copies, waits for them, and re-layouts: 14.4 us -> 16.6 us
  transfers between devices with their start and end apart: 6 -> 21, of which waited for: 3 -> 7; matrix products, arithmetic and copies ran while one was open for 26% -> 25% of each run, Pallas kernels for 0% -> 0%
where the time goes in v1:
time: 332 us; the launch traced here: 331 us
  waiting for transfers between devices  117 us (35%)
  local copies, waits for them, and re-layouts  74.5 us (22%)
  starting transfers between devices  45.8 us (14%)
  blocking collectives  41.3 us (12%)
  other arithmetic  24.4 us (7%)
  between operations  15.8 us (5%)
  matrix products  11.8 us (4%)
    psum x1, waiting for transfers between devices, on_device(): shared_gate_pre, shared_up_pre = lax.psum((sgate_part, sup_part), 'tp')  42.6 us
    all_to_all x1, waiting for transfers between devices, on_device(): lax.all_to_all(expert_out, 'tp', split_axis=1, concat_axis=0, tiled=True)  38.6 us
    all_to_all x1, blocking collectives, on_device(): lax.all_to_all(up_cast, 'tp', split_axis=0, concat_axis=2, tiled=True)  35.6 us
    ppermute x15, starting transfers between devices, spots_supply(): lax.ppermute(next_value, along_axis, perm=[(s, s ^ dev_j) for s in range(...  34.9 us
    all_to_all x1, waiting for transfers between devices, on_device(): lax.all_to_all(down_cast, 'tp', split_axis=0, concat_axis=2, tiled=True)  22.6 us
    unnamed x34, local copies, waits for them, and re-layouts  16.6 us
    ppermute x15, waiting for transfers between devices, spots_supply(): lax.ppermute(next_value, along_axis, perm=[(s, s ^ dev_j) for s in range(...  12.7 us
    gather x16, local copies, waits for them, and re-layouts, add_expert(): jnp.take(source_rows, jnp.maximum(source_position, 0), axis=0)  11.7 us
  transfers between devices with their start and end apart: 21, of which 7 were waited for; matrix products, arithmetic and copies ran while one was open for 25% of the time, Pallas kernels for 0%

profile of v1, /device:TPU:0, one launch (start us, length us, event | category | flops | bytes accessed | tf_op | source)
XLA Modules:
  0.0 330.8 jit_solution(9658037919233512335)
XLA Ops:
  8.2 2.5 multiply_convert_fusion
  11.8 3.3 constant_dynamic-slice_fusion
  15.1 3.0 collective-permute-start
  23.0 2.5 collective-permute-start.5
  29.4 2.6 collective-permute-start.7
  41.5 3.1 collective-permute-start.11
  44.8 7.1 %collective-permute-done.7 = bf16[1,252,128]{2,0,1:T(2,128)(2,1)S(1)} collective-permute-done((bf16[1,252,128]{2,0,1:T(2,128)(2,1)}, bf16[1,252,128]{2,0,1:T(2,128)(2,1)S(1)}, u32[]{:S(2)}, u32[]{:S(2)}) %collective-permute-start.7) | collective-permute-done | bytes 64544 | tf_op jit(solution)/shard_map/ppermute | solution.py:26
  51.9 2.6 collective-permute-start.12
  58.3 2.9 collective-permute-done.9
  61.1 6.3 %collective-permute-start.14 = (bf16[1,252,128]{2,0,1:T(2,128)(2,1)S(1)}, bf16[1,252,128]{2,0,1:T(2,128)(2,1)S(1)}, u32[]{:S(2)}, u32[]{:S(2)}) collective-permute-start(bf16[1,252,128]{2,0,1:T(2,128)(2,1)S(1)} %get-tuple-element.166), channel_id=1, source_target_pairs={{0,15},{1,14},{2,13},{3,12},{4,11},{5,10},{6,9},{7,8},{8,7},{9,6},... | collective-permute-start | bytes 193544 | tf_op jit(solution)/shard_map/ppermute | solution.py:26
  72.4 35.6 %all_to_all.49 = bf16[16,252,128]{2,1,0:T(8,128)(2,1)S(1)} all-to-all(bf16[16,252,128]{2,1,0:T(8,128)(2,1)S(1)} %copy.72), channel_id=1, replica_groups=mesh['fs'=2,'tp'=16] {'tp'}, dimensions={0} | all-to-all | bytes 2064384 | tf_op jit(solution)/shard_map/all_to_all | solution.py:64
  108.5 3.7 %copy.74 = bf16[1,252,2048]{2,0,1:T(2,128)(2,1)} copy(bf16[1,252,2048]{1,2,0:T(8,128)(2,1)S(1)} %bitcast.67) | data formatting | bytes 2064384 | tf_op jit(solution)/shard_map/all_to_all | solution.py:64
  113.7 3.8 %all-to-all-start.1 = ((bf16[16,252,128]{2,1,0:T(8,128)(2,1)}), bf16[16,252,128]{2,1,0:T(8,128)(2,1)S(1)}, u32[]{:S(2)}, u32[]{:S(2)}) async-start(bf16[16,252,128]{2,1,0:T(8,128)(2,1)} %copy.75), calls=%async_computation.1 | async-start | bytes 2097152 | tf_op jit(solution)/shard_map/all_to_all | solution.py:65
  118.3 22.6 %all-to-all-done.1 = bf16[16,252,128]{2,1,0:T(8,128)(2,1)S(1)} async-done(((bf16[16,252,128]{2,1,0:T(8,128)(2,1)}), bf16[16,252,128]{2,1,0:T(8,128)(2,1)S(1)}, u32[]{:S(2)}, u32[]{:S(2)}) %all-to-all-start.1) | async-done | bytes 1032224 | tf_op jit(solution)/shard_map/all_to_all | solution.py:65
  141.5 3.9 %copy.77 = bf16[1,252,2048]{2,0,1:T(2,128)(2,1)} copy(bf16[1,252,2048]{1,2,0:T(8,128)(2,1)S(1)} %bitcast.68) | data formatting | bytes 2064384 | tf_op jit(solution)/shard_map/all_to_all | solution.py:65
  147.7 5.1 %copy.80 = bf16[1,504,2048]{2,1,0:T(8,128)(2,1)} copy(bf16[1,504,2048]{2,0,1:T(2,128)(2,1)} %all-gather.10.cloned.1.call-done) | data formatting | bytes 4128768
  152.7 4.1 %copy.81 = bf16[1,504,2048]{2,1,0:T(8,128)(2,1)S(1)} copy(bf16[1,504,2048]{2,0,1:T(2,128)(2,1)} %all-gather.12.cloned.1.call-done) | data formatting | bytes 4128768
  159.7 9.0 %copy.87 = bf16[1,504,2048]{1,2,0:T(8,128)(2,1)S(1)} copy(bf16[1,504,2048]{2,0,1:T(2,128)(2,1)} %all-gather.14.cloned.1.call-done) | data formatting | bytes 4128768 | tf_op jit(solution)/shard_map/dot_general | solution.py:106
  168.7 5.8 %fusion.13 = f32[256,16,128]{2,0,1:T(8,128)} fusion(bf16[16,128,504]{2,1,0:T(8,128)(2,1)S(1)} %bitcast.70, f32[256,504]{0,1:T(8,128)} %fusion.2, bf16[1,504,2048]{2,1,0:T(8,128)(2,1)} %copy.80, bf16[256,2048]{1,0:T(8,128)(2,1)} %copy-done.4, pred[256]{0:T(512)(128)(4,1)S(1)} %compare_and_fusion), kind=kOutput, calls=%fused_computation.27 | convolution fusion | flops 1058263040 | bytes 7790848 | tf_op jit(solution)/shard_map/dot_general | solution.py:106
  174.6 6.6 %all-to-all-start.2 = ((f32[256,16,128]{2,0,1:T(8,128)}), f32[256,16,128]{2,0,1:T(8,128)S(1)}, u32[]{:S(2)}, u32[]{:S(2)}) async-start(f32[256,16,128]{2,0,1:T(8,128)} %fusion.13), calls=%async_computation.2 | async-start | bytes 4194304 | tf_op jit(solution)/shard_map/all_to_all | solution.py:108
  189.5 4.8 %copy.82 = bf16[1,504,2048]{2,1,0:T(8,128)(2,1)} copy(bf16[1,504,2048]{2,0,1:T(2,128)(2,1)} %all-gather.14.cloned.1.call-done) | data formatting | bytes 4128768
  194.2 38.6 %all-to-all-done.2 = f32[256,16,128]{2,0,1:T(8,128)S(1)} async-done(((f32[256,16,128]{2,0,1:T(8,128)}), f32[256,16,128]{2,0,1:T(8,128)S(1)}, u32[]{:S(2)}, u32[]{:S(2)}) %all-to-all-start.2) | async-done | bytes 2097184 | tf_op jit(solution)/shard_map/all_to_all | solution.py:108
  232.8 46.1 %while.13 = (s32[]{:T(128)}, f32[256,128]{1,0:T(8,128)S(1)}, s32[16]{0:T(128)S(1)}, s32[256,8]{0,1:T(8,128)S(1)}, f32[16,256,128]{2,1,0:T(8,128)S(1)}, /*index=5...) while((s32[]{:T(128)}, f32[256,128]{1,0:T(8,128)S(1)}, s32[16]{0:T(128)S(1)}, ...), condition=%wide.region_11.12_spmd.clone, body=%wide.region_6.11_spmd.clone.sunk | while | flops 206342 | bytes 952776 | solution.py:123
  278.9 42.6 %all-reduce.3.cloned.1.call-done = (f32[256,504]{0,1:T(8,128)}, f32[256,504]{0,1:T(8,128)}) async-done(((f32[256,504]{0,1:T(8,128)}, f32[256,504]{0,1:T(8,128)}), (f32[256,504]{0,1:T(8,128)}, f32[256,504]{0,1:T(8,128)})) %all-reduce.3.cloned.1.call-update) | async-done | bytes 1032208 | tf_op jit(solution)/shard_map/psum | solution.py:104
  (321 shorter events, 92.2 us)
Async XLA Ops:
  8.0 139.6 %all-gather.10.cloned.1.call-start = ((), (), s32[]{:S(2)}) async-start(), calls=%async_computation.3 | async-start | bytes 6193152 | tf_op jit(solution)/shard_map/all_gather | solution.py:91
  15.1 7.9 %collective-permute-start = (bf16[1,252,128]{2,0,1:T(2,128)(2,1)}, bf16[1,252,128]{2,0,1:T(2,128)(2,1)}, u32[]{:S(2)}, u32[]{:S(2)}) collective-permute-start(bf16[1,252,128]{2,0,1:T(2,128)(2,1)} %get-tuple-element.180), channel_id=1, source_target_pairs={{0,1},{1,0},{2,3},{3,2},{4,5},{5,4},{6,7},{7,6},{8,9},{9,8},{10,11... | collective-permute-start | bytes 193544 | tf_op jit(solution)/shard_map/ppermute | solution.py:26
  18.0 8.6 %collective-permute-start.1 = (bf16[1,252,128]{2,0,1:T(2,128)(2,1)}, bf16[1,252,128]{2,0,1:T(2,128)(2,1)}, u32[]{:S(2)}, u32[]{:S(2)}) collective-permute-start(bf16[1,252,128]{2,0,1:T(2,128)(2,1)} %get-tuple-element.179), channel_id=1, source_target_pairs={{0,2},{1,3},{2,0},{3,1},{4,6},{5,7},{6,4},{7,5},{8,10},{9,11},{10,... | collective-permute-start | bytes 193544 | tf_op jit(solution)/shard_map/ppermute | solution.py:26
  19.5 9.8 %collective-permute-start.2 = (bf16[1,252,128]{2,0,1:T(2,128)(2,1)}, bf16[1,252,128]{2,0,1:T(2,128)(2,1)}, u32[]{:S(2)}, u32[]{:S(2)}) collective-permute-start(bf16[1,252,128]{2,0,1:T(2,128)(2,1)} %get-tuple-element.178), channel_id=1, source_target_pairs={{0,3},{1,2},{2,1},{3,0},{4,7},{5,6},{6,5},{7,4},{8,11},{9,10},{10,... | collective-permute-start | bytes 193544 | tf_op jit(solution)/shard_map/ppermute | solution.py:26
  19.5 13.6 %collective-permute-start.3 = (bf16[1,252,128]{2,0,1:T(2,128)(2,1)}, bf16[1,252,128]{2,0,1:T(2,128)(2,1)}, u32[]{:S(2)}, u32[]{:S(2)}) collective-permute-start(bf16[1,252,128]{2,0,1:T(2,128)(2,1)} %get-tuple-element.177), channel_id=1, source_target_pairs={{0,4},{1,5},{2,6},{3,7},{4,0},{5,1},{6,2},{7,3},{8,12},{9,13},{10,... | collective-permute-start | bytes 193544 | tf_op jit(solution)/shard_map/ppermute | solution.py:26
  21.6 14.9 %collective-permute-start.4 = (bf16[1,252,128]{2,0,1:T(2,128)(2,1)}, bf16[1,252,128]{2,0,1:T(2,128)(2,1)}, u32[]{:S(2)}, u32[]{:S(2)}) collective-permute-start(bf16[1,252,128]{2,0,1:T(2,128)(2,1)} %get-tuple-element.176), channel_id=1, source_target_pairs={{0,5},{1,4},{2,7},{3,6},{4,1},{5,0},{6,3},{7,2},{8,13},{9,12},{10,... | collective-permute-start | bytes 193544 | tf_op jit(solution)/shard_map/ppermute | solution.py:26
  23.0 16.2 %collective-permute-start.5 = (bf16[1,252,128]{2,0,1:T(2,128)(2,1)}, bf16[1,252,128]{2,0,1:T(2,128)(2,1)S(1)}, u32[]{:S(2)}, u32[]{:S(2)}) collective-permute-start(bf16[1,252,128]{2,0,1:T(2,128)(2,1)} %get-tuple-element.175), channel_id=1, source_target_pairs={{0,6},{1,7},{2,4},{3,5},{4,2},{5,3},{6,0},{7,1},{8,14},{9,15},{10,... | collective-permute-start | bytes 193544 | tf_op jit(solution)/shard_map/ppermute | solution.py:26
  26.6 14.9 %collective-permute-start.6 = (bf16[1,252,128]{2,0,1:T(2,128)(2,1)}, bf16[1,252,128]{2,0,1:T(2,128)(2,1)S(1)}, u32[]{:S(2)}, u32[]{:S(2)}) collective-permute-start(bf16[1,252,128]{2,0,1:T(2,128)(2,1)} %get-tuple-element.174), channel_id=1, source_target_pairs={{0,7},{1,6},{2,5},{3,4},{4,3},{5,2},{6,1},{7,0},{8,15},{9,14},{10,... | collective-permute-start | bytes 193544 | tf_op jit(solution)/shard_map/ppermute | solution.py:26
  29.4 22.5 %collective-permute-start.7 = (bf16[1,252,128]{2,0,1:T(2,128)(2,1)}, bf16[1,252,128]{2,0,1:T(2,128)(2,1)S(1)}, u32[]{:S(2)}, u32[]{:S(2)}) collective-permute-start(bf16[1,252,128]{2,0,1:T(2,128)(2,1)} %get-tuple-element.173), channel_id=1, source_target_pairs={{0,8},{1,9},{2,10},{3,11},{4,12},{5,13},{6,14},{7,15},{8,0},{9,1},... | collective-permute-start | bytes 193544 | tf_op jit(solution)/shard_map/ppermute | solution.py:26
  33.1 22.5 %collective-permute-start.8 = (bf16[1,252,128]{2,0,1:T(2,128)(2,1)}, bf16[1,252,128]{2,0,1:T(2,128)(2,1)S(1)}, u32[]{:S(2)}, u32[]{:S(2)}) collective-permute-start(bf16[1,252,128]{2,0,1:T(2,128)(2,1)} %get-tuple-element.172), channel_id=1, source_target_pairs={{0,9},{1,8},{2,11},{3,10},{4,13},{5,12},{6,15},{7,14},{8,1},{9,0},... | collective-permute-start | bytes 193544 | tf_op jit(solution)/shard_map/ppermute | solution.py:26
  36.5 24.6 %collective-permute-start.9 = (bf16[1,252,128]{2,0,1:T(2,128)(2,1)}, bf16[1,252,128]{2,0,1:T(2,128)(2,1)S(1)}, u32[]{:S(2)}, u32[]{:S(2)}) collective-permute-start(bf16[1,252,128]{2,0,1:T(2,128)(2,1)} %get-tuple-element.171), channel_id=1, source_target_pairs={{0,10},{1,11},{2,8},{3,9},{4,14},{5,15},{6,12},{7,13},{8,2},{9,3},... | collective-permute-start | bytes 193544 | tf_op jit(solution)/shard_map/ppermute | solution.py:26
  39.2 28.5 %collective-permute-start.10 = (bf16[1,252,128]{2,0,1:T(2,128)(2,1)}, bf16[1,252,128]{2,0,1:T(2,128)(2,1)S(1)}, u32[]{:S(2)}, u32[]{:S(2)}) collective-permute-start(bf16[1,252,128]{2,0,1:T(2,128)(2,1)} %get-tuple-element.170), channel_id=1, source_target_pairs={{0,11},{1,10},{2,9},{3,8},{4,15},{5,14},{6,13},{7,12},{8,3},{9,2},... | collective-permute-start | bytes 193544 | tf_op jit(solution)/shard_map/ppermute | solution.py:26
  41.5 26.4 %collective-permute-start.11 = (bf16[1,252,128]{2,0,1:T(2,128)(2,1)}, bf16[1,252,128]{2,0,1:T(2,128)(2,1)S(1)}, u32[]{:S(2)}, u32[]{:S(2)}) collective-permute-start(bf16[1,252,128]{2,0,1:T(2,128)(2,1)} %get-tuple-element.169), channel_id=1, source_target_pairs={{0,12},{1,13},{2,14},{3,15},{4,8},{5,9},{6,10},{7,11},{8,4},{9,5},... | collective-permute-start | bytes 193544 | tf_op jit(solution)/shard_map/ppermute | solution.py:26
  51.9 16.3 %collective-permute-start.12 = (bf16[1,252,128]{2,0,1:T(2,128)(2,1)S(1)}, bf16[1,252,128]{2,0,1:T(2,128)(2,1)S(1)}, u32[]{:S(2)}, u32[]{:S(2)}) collective-permute-start(bf16[1,252,128]{2,0,1:T(2,128)(2,1)S(1)} %get-tuple-element.168), channel_id=1, source_target_pairs={{0,13},{1,12},{2,15},{3,14},{4,9},{5,8},{6,11},{7,10},{8,5},{9,4},... | collective-permute-start | bytes 193544 | tf_op jit(solution)/shard_map/ppermute | solution.py:26
  55.6 12.8 %collective-permute-start.13 = (bf16[1,252,128]{2,0,1:T(2,128)(2,1)S(1)}, bf16[1,252,128]{2,0,1:T(2,128)(2,1)S(1)}, u32[]{:S(2)}, u32[]{:S(2)}) collective-permute-start(bf16[1,252,128]{2,0,1:T(2,128)(2,1)S(1)} %get-tuple-element.167), channel_id=1, source_target_pairs={{0,14},{1,15},{2,12},{3,13},{4,10},{5,11},{6,8},{7,9},{8,6},{9,7},... | collective-permute-start | bytes 193544 | tf_op jit(solution)/shard_map/ppermute | solution.py:26
  61.1 9.4 %collective-permute-start.14 = (bf16[1,252,128]{2,0,1:T(2,128)(2,1)S(1)}, bf16[1,252,128]{2,0,1:T(2,128)(2,1)S(1)}, u32[]{:S(2)}, u32[]{:S(2)}) collective-permute-start(bf16[1,252,128]{2,0,1:T(2,128)(2,1)S(1)} %get-tuple-element.166), channel_id=1, source_target_pairs={{0,15},{1,14},{2,13},{3,12},{4,11},{5,10},{6,9},{7,8},{8,7},{9,6},... | collective-permute-start | bytes 193544 | tf_op jit(solution)/shard_map/ppermute | solution.py:26
  72.0 80.7 %all-gather.12.cloned.1.call-start = ((), (), s32[]{:S(2)}) async-start(), calls=%async_computation.4 | async-start | bytes 6193152 | tf_op jit(solution)/shard_map/all_gather | solution.py:92
  113.7 27.3 %all-to-all-start.1 = ((bf16[16,252,128]{2,1,0:T(8,128)(2,1)}), bf16[16,252,128]{2,1,0:T(8,128)(2,1)S(1)}, u32[]{:S(2)}, u32[]{:S(2)}) async-start(bf16[16,252,128]{2,1,0:T(8,128)(2,1)} %copy.75), calls=%async_computation.1 | async-start | bytes 2097152 | tf_op jit(solution)/shard_map/all_to_all | solution.py:65
  117.5 42.2 %all-gather.14.cloned.1.call-start = ((), (), s32[]{:S(2)}) async-start(), calls=%async_computation.5 | async-start | bytes 6193152 | tf_op jit(solution)/shard_map/all_gather | solution.py:93
  147.6 9.2 %copy-start.4 = (bf16[256,2048]{1,0:T(8,128)(2,1)}, bf16[256,2048]{1,0:T(8,128)(2,1)S(1)}, u32[]{:S(2)}) copy-start(bf16[256,2048]{1,0:T(8,128)(2,1)S(1)} %gather_fusion.1) | copy-start | bytes 3145732
  174.6 58.3 %all-to-all-start.2 = ((f32[256,16,128]{2,0,1:T(8,128)}), f32[256,16,128]{2,0,1:T(8,128)S(1)}, u32[]{:S(2)}, u32[]{:S(2)}) async-start(f32[256,16,128]{2,0,1:T(8,128)} %fusion.13), calls=%async_computation.2 | async-start | bytes 4194304 | tf_op jit(solution)/shard_map/all_to_all | solution.py:108
  181.2 140.3 %all-reduce.3.cloned.1.call-start = ((), (), s32[]{:S(2)}) async-start(), calls=%async_computation.6 | async-start | bytes 2064384 | tf_op jit(solution)/shard_map/psum | solution.py:104
  183.3 10.9 %copy-start.5 = (bf16[504,128]{1,0:T(8,128)(2,1)}, bf16[504,128]{1,0:T(8,128)(2,1)S(1)}, u32[]{:S(2)}) copy-start(bf16[504,128]{1,0:T(8,128)(2,1)S(1)} %reshape.181) | copy-start | bytes 387076
  189.4 132.1 %copy-start.11 = (bf16[504,128]{1,0:T(8,128)(2,1)}, bf16[504,128]{1,0:T(8,128)(2,1)S(1)}, u32[]{:S(2)}) copy-start(bf16[504,128]{1,0:T(8,128)(2,1)S(1)} %reshape.185) | copy-start | bytes 387076
  (11 other events, 55.4 us)
Sparse Core Ops, SparseCore 0:
  72.2 18.2 all-gather.9
  112.4 11.7 all-gather.11
  145.6 13.8 all-gather.13
Sparse Core Ops, SparseCore 1:
  187.5 133.9 all-reduce.2
